TPU v7x, 32 devices: a whole 2x2x4 slice. The times are simulated.
32 devices in a mesh: kv: 16 (over z, y, x), tp: 2 (over core).
Axes of the slice: x: 2, y: 2, z: 4, core: 2. Of those that a mesh axis runs over, the one named last changes fastest.
Arguments:
- tokens: bfloat16 [64, 4, 2048], P('kv', None, 'tp'), may hold values from -6 to 6
- input_gain: float32 [2048], replicated, may hold values from 0.1 to 1.9
- gate_weight: bfloat16 [2048, 4096], P('kv', 'tp'), may hold values from -0.125 to 0.125
- value_weight: bfloat16 [2048, 4096], P('kv', 'tp'), may hold values from -0.125 to 0.125
- write_weight: bfloat16 [2048, 1024], P('kv', 'tp'), may hold values from -0.125 to 0.125
- read_weight: bfloat16 [2048, 1024], P('kv', 'tp'), may hold values from -0.125 to 0.125
- step_weight: bfloat16 [2048, 64], replicated, may hold values from -0.125 to 0.125
- conv_value: float32 [4, 4096], P(None, 'tp'), may hold values from -3 to 3
- conv_write: float32 [4, 1024], P(None, 'tp'), may hold values from -3 to 3
- conv_read: float32 [4, 1024], P(None, 'tp'), may hold values from -3 to 3
- step_bias: float32 [64], P('tp'), may hold values from -4 to -1
- decay_log: float32 [64], P('tp'), may hold values from 0 to 2.8
- skip_gain: float32 [64], P('tp'), may hold values from 0.5 to 1.5
- output_gain: float32 [4096], P('tp'), may hold values from 0.1 to 1.9
- out_weight: bfloat16 [4096, 2048], P('tp', 'kv'), may hold values from -0.09375 to 0.09375
- base_state: float32 [64, 64, 64, 128], P('kv', 'tp'), may hold values from -2 to 2
- past_value: bfloat16 [64, 7, 4096], P('kv', None, 'tp'), may hold values from -6 to 6
- past_write: bfloat16 [64, 7, 1024], P('kv', None, 'tp'), may hold values from -6 to 6
- past_read: bfloat16 [64, 7, 1024], P('kv', None, 'tp'), may hold values from -6 to 6
- past_step: bfloat16 [64, 4, 64], P('kv', None, 'tp'), may hold values from -4 to 4
- accepted: int32 [64], P('kv'), may hold values from 1 to 4
Outputs:
- mixed: bfloat16 [64, 4, 2048], P('kv', None, 'tp')
- root_state: float32 [64, 64, 64, 128], P('kv', 'tp')
- next_value: bfloat16 [64, 7, 4096], P('kv', None, 'tp')
- next_write: bfloat16 [64, 7, 1024], P('kv', None, 'tp')
- next_read: bfloat16 [64, 7, 1024], P('kv', None, 'tp')
- next_step: bfloat16 [64, 4, 64], P('kv', None, 'tp')
Inputs may be any that keep to these rules, and one draw needn't show every extreme that they name: Every entry of `accepted` is an integer from 1 to 4 (at least one of the last step's proposals is always accepted).
All inputs are finite; a program needn't handle non-finite values.
Results may differ from a plain program's by a relative error of at most 0.018.
Values may be sent and summed in bfloat16 or wider, within the bound.
No kernel may reach another device: no remote copies, remote signals or barrier semaphores. Data moves between devices by JAX's collectives and lax.ppermute only.
A program may use at most 64 MiB of HBM per device.

v0:
```python
import jax
import jax.numpy as jnp
from jax import lax
from jax.sharding import PartitionSpec as P

STATE_DIM = 128
CONV_W = 4
EPSILON = 1e-06


def causal_conv(rows, kernel):
    width = kernel.shape[0]
    count = rows.shape[0] - width + 1
    total = kernel[0] * rows[0:count]
    for offset in range(1, width):
        total = total + kernel[offset] * rows[offset : offset + count]
    return total


def advance(
    past_x,
    past_b,
    past_c,
    past_dt,
    taken,
    state_zero,
    value_now,
    write_now,
    read_now,
    gate_now,
    step_now,
    conv_value,
    conv_write,
    conv_read,
    step_bias,
    decay_log,
    skip_gain,
    output_gain,
):
    highest = lax.Precision.HIGHEST
    proposals = value_now.shape[0]
    head_count = step_bias.shape[0]
    group_count = write_now.shape[1] // STATE_DIM
    per_group = head_count // group_count
    head_width = value_now.shape[1] // head_count
    rate = jnp.exp(decay_log)
    prev_x = jax.nn.silu(causal_conv(past_x.astype(jnp.float32), conv_value)).reshape(
        proposals, head_count, head_width
    )
    prev_b = jax.nn.silu(causal_conv(past_b.astype(jnp.float32), conv_write)).reshape(
        proposals, group_count, STATE_DIM
    )
    prev_b = jnp.repeat(prev_b, per_group, axis=1)
    prev_dt = jax.nn.softplus(past_dt.astype(jnp.float32) + step_bias)
    live = (jnp.arange(proposals, dtype=jnp.int32) < taken)[:, None]
    prev_log = jnp.where(live, -rate * prev_dt, jnp.zeros_like(prev_dt))
    total_log = jnp.sum(prev_log, axis=0)
    tail_log = total_log - jnp.cumsum(prev_log, axis=0)
    weight_now = jnp.where(live, jnp.exp(tail_log) * prev_dt, jnp.zeros_like(prev_dt))
    root = jnp.exp(total_log)[:, None, None] * state_zero + jnp.einsum(
        "sh,shp,shn->hpn", weight_now, prev_x, prev_b, precision=highest
    )
    window_x = jnp.concatenate(
        [lax.dynamic_slice_in_dim(past_x, taken, CONV_W - 1, 0), value_now], axis=0
    )
    window_b = jnp.concatenate(
        [lax.dynamic_slice_in_dim(past_b, taken, CONV_W - 1, 0), write_now], axis=0
    )
    window_c = jnp.concatenate(
        [lax.dynamic_slice_in_dim(past_c, taken, CONV_W - 1, 0), read_now], axis=0
    )
    cur_x = jax.nn.silu(causal_conv(window_x.astype(jnp.float32), conv_value)).reshape(
        proposals, head_count, head_width
    )
    cur_b = jax.nn.silu(causal_conv(window_b.astype(jnp.float32), conv_write)).reshape(
        proposals, group_count, STATE_DIM
    )
    cur_c = jax.nn.silu(causal_conv(window_c.astype(jnp.float32), conv_read)).reshape(
        proposals, group_count, STATE_DIM
    )
    cur_b = jnp.repeat(cur_b, per_group, axis=1)
    cur_c = jnp.repeat(cur_c, per_group, axis=1)
    cur_dt = jax.nn.softplus(step_now.astype(jnp.float32) + step_bias)
    logs = jnp.cumsum(-rate * cur_dt, axis=0)
    carried = jnp.einsum("thn,hpn->thp", cur_c, root, precision=highest) * jnp.exp(logs)[:, :, None]
    lower = (jnp.arange(proposals)[:, None] >= jnp.arange(proposals)[None, :])[:, :, None]
    diff = logs[:, None, :] - logs[None, :, :]
    decay = jnp.where(
        lower, jnp.exp(jnp.where(lower, diff, jnp.zeros_like(diff))), jnp.zeros_like(diff)
    )
    scores = (
        jnp.einsum("thn,shn->tsh", cur_c, cur_b, precision=highest) * decay * cur_dt[None, :, :]
    )
    inner = jnp.einsum("tsh,shp->thp", scores, cur_x, precision=highest)
    mixed = carried + inner + skip_gain[None, :, None] * cur_x
    gated = mixed.reshape(proposals, -1) * jax.nn.silu(gate_now.astype(jnp.float32))
    grouped = gated.reshape(proposals, group_count, -1)
    grouped = grouped * lax.rsqrt(jnp.mean(grouped * grouped, axis=-1, keepdims=True) + EPSILON)
    result = (grouped.reshape(proposals, -1) * output_gain).astype(jnp.bfloat16)
    return (result, root, window_x, window_b, window_c)


def on_device(
    tokens,
    input_gain,
    gate_weight,
    value_weight,
    write_weight,
    read_weight,
    step_weight,
    conv_value,
    conv_write,
    conv_read,
    step_bias,
    decay_log,
    skip_gain,
    output_gain,
    out_weight,
    base_state,
    past_value,
    past_write,
    past_read,
    past_step,
    accepted,
):
    whole = lax.all_gather(tokens, "tp", axis=2, tiled=True)
    seq_local, proposals, width = whole.shape
    rows = whole.astype(jnp.float32)
    normed = (
        rows * lax.rsqrt(jnp.mean(rows * rows, axis=-1, keepdims=True) + EPSILON) * input_gain
    ).astype(jnp.bfloat16)
    flat = normed.reshape(seq_local * proposals, width)
    token_count = flat.shape[0]
    head_count = step_bias.shape[0]
    own_step = lax.dynamic_slice_in_dim(
        step_weight, lax.axis_index("tp") * head_count, head_count, 1
    )
    step_now = jnp.dot(flat, own_step, preferred_element_type=jnp.float32).astype(jnp.bfloat16)
    slabs = (
        lax.all_to_all(gate_weight, "kv", split_axis=1, concat_axis=0, tiled=True),
        lax.all_to_all(value_weight, "kv", split_axis=1, concat_axis=0, tiled=True),
        lax.all_to_all(write_weight, "kv", split_axis=1, concat_axis=0, tiled=True),
        lax.all_to_all(read_weight, "kv", split_axis=1, concat_axis=0, tiled=True),
    )
    spans = [slab.shape[1] for slab in slabs]
    narrow = jnp.concatenate(slabs, axis=1)
    everyone = jnp.dot(
        lax.all_gather(flat, "kv", axis=0, tiled=True), narrow, preferred_element_type=jnp.float32
    ).astype(jnp.bfloat16)
    returned = lax.all_to_all(everyone, "kv", split_axis=0, concat_axis=1, tiled=True)
    ranks = lax.axis_size("kv")
    returned = returned.reshape(token_count, ranks, sum(spans))
    pieces_out = []
    offset = 0
    for span in spans:
        pieces_out.append(returned[:, :, offset : offset + span].reshape(token_count, ranks * span))
        offset = offset + span
    gate_now, value_now, write_now, read_now = pieces_out
    shaped = [
        item.reshape(seq_local, proposals, item.shape[1])
        for item in (value_now, write_now, read_now, gate_now, step_now)
    ]
    stepper = jax.vmap(advance, in_axes=(0,) * 11 + (None,) * 7)
    normal_out, root_state, next_value, next_write, next_read = stepper(
        past_value,
        past_write,
        past_read,
        past_step,
        accepted,
        base_state,
        shaped[0],
        shaped[1],
        shaped[2],
        shaped[3],
        shaped[4],
        conv_value,
        conv_write,
        conv_read,
        step_bias,
        decay_log,
        skip_gain,
        output_gain,
    )
    flat_y = normal_out.reshape(token_count, -1)
    partial_sum = jnp.dot(
        flat_y,
        lax.all_gather(out_weight, "kv", axis=1, tiled=True),
        preferred_element_type=jnp.float32,
    )
    summed = lax.psum_scatter(
        partial_sum.astype(jnp.bfloat16), "tp", scatter_dimension=1, tiled=True
    ).astype(jnp.float32)
    mixed = summed.astype(jnp.bfloat16).reshape(seq_local, proposals, summed.shape[1])
    return (mixed, root_state, next_value, next_write, next_read, shaped[4])


def solution(mesh):
    return jax.shard_map(
        on_device,
        mesh=mesh,
        in_specs=(
            P("kv", None, "tp"),
            P(),
            P("kv", "tp"),
            P("kv", "tp"),
            P("kv", "tp"),
            P("kv", "tp"),
            P(),
            P(None, "tp"),
            P(None, "tp"),
            P(None, "tp"),
            P("tp"),
            P("tp"),
            P("tp"),
            P("tp"),
            P("tp", "kv"),
            P("kv", "tp", None, None),
            P("kv", None, "tp"),
            P("kv", None, "tp"),
            P("kv", None, "tp"),
            P("kv", None, "tp"),
            P("kv"),
        ),
        out_specs=(
            P("kv", None, "tp"),
            P("kv", "tp", None, None),
            P("kv", None, "tp"),
            P("kv", None, "tp"),
            P("kv", None, "tp"),
            P("kv", None, "tp"),
        ),
        check_vma=False,
    )
```

profile of v0, /device:TPU:0, one launch (start us, length us, event | category | flops | bytes accessed | tf_op | source)
XLA Modules:
  0.0 240.1 jit_solution(14722465819496785952)
XLA Ops:
  7.3 2.3 all_gather.9
  9.8 0.8 fusion.18
  10.6 0.6 reshape.162
  11.3 0.7 all-gather.5.cloned.1.call-update
  12.0 1.7 copy.196
  13.7 8.2 %all-to-all-start.2 = ((bf16[128,16,32]{0,2,1:T(8,128)(2,1)}), bf16[128,16,32]{0,2,1:T(8,128)(2,1)S(1)}, u32[]{:S(2)}, u32[]{:S(2)}) async-start(bf16[128,16,32]{0,2,1:T(8,128)(2,1)} %bitcast.19), calls=%async_computation.2 | async-start | bytes 262144 | tf_op jit(solution)/shard_map/all_to_all | solution.py:142
  21.9 1.7 copy.198
  23.6 6.5 %all-to-all-done.2 = bf16[128,16,32]{0,2,1:T(8,128)(2,1)S(1)} async-done(((bf16[128,16,32]{0,2,1:T(8,128)(2,1)}), bf16[128,16,32]{0,2,1:T(8,128)(2,1)S(1)}, u32[]{:S(2)}, u32[]{:S(2)}) %all-to-all-start.2) | async-done | bytes 131104 | tf_op jit(solution)/shard_map/all_to_all | solution.py:142
  30.1 3.5 %all-to-all-start.3 = ((bf16[128,16,32]{0,2,1:T(8,128)(2,1)}), bf16[128,16,32]{0,2,1:T(8,128)(2,1)S(1)}, u32[]{:S(2)}, u32[]{:S(2)}) async-start(bf16[128,16,32]{0,2,1:T(8,128)(2,1)} %bitcast.22), calls=%async_computation.3 | async-start | bytes 262144 | tf_op jit(solution)/shard_map/all_to_all | solution.py:143
  33.6 2.0 copy.192
  35.6 5.7 %all-to-all-done.3 = bf16[128,16,32]{0,2,1:T(8,128)(2,1)S(1)} async-done(((bf16[128,16,32]{0,2,1:T(8,128)(2,1)}), bf16[128,16,32]{0,2,1:T(8,128)(2,1)S(1)}, u32[]{:S(2)}, u32[]{:S(2)}) %all-to-all-start.3) | async-done | bytes 131104 | tf_op jit(solution)/shard_map/all_to_all | solution.py:143
  41.4 3.6 %all-to-all-start = ((bf16[128,16,128]{0,2,1:T(8,128)(2,1)}), bf16[128,16,128]{0,2,1:T(8,128)(2,1)S(1)}, u32[]{:S(2)}, u32[]{:S(2)}) async-start(bf16[128,16,128]{0,2,1:T(8,128)(2,1)} %bitcast.13), calls=%async_computation | async-start | bytes 1048576 | tf_op jit(solution)/shard_map/all_to_all | solution.py:140
  45.0 1.0 copy.194
  46.3 13.3 %all-to-all-done = bf16[128,16,128]{0,2,1:T(8,128)(2,1)S(1)} async-done(((bf16[128,16,128]{0,2,1:T(8,128)(2,1)}), bf16[128,16,128]{0,2,1:T(8,128)(2,1)S(1)}, u32[]{:S(2)}, u32[]{:S(2)}) %all-to-all-start) | async-done | bytes 524320 | tf_op jit(solution)/shard_map/all_to_all | solution.py:140
  59.6 3.9 %all-to-all-start.1 = ((bf16[128,16,128]{0,2,1:T(8,128)(2,1)}), bf16[128,16,128]{0,2,1:T(8,128)(2,1)S(1)}, u32[]{:S(2)}, u32[]{:S(2)}) async-start(bf16[128,16,128]{0,2,1:T(8,128)(2,1)} %bitcast.16), calls=%async_computation.1 | async-start | bytes 1048576 | tf_op jit(solution)/shard_map/all_to_all | solution.py:141
  63.8 0.8 gather_fusion.1
  65.5 0.6 gather_fusion
  67.2 12.8 %all-to-all-done.1 = bf16[128,16,128]{0,2,1:T(8,128)(2,1)S(1)} async-done(((bf16[128,16,128]{0,2,1:T(8,128)(2,1)}), bf16[128,16,128]{0,2,1:T(8,128)(2,1)S(1)}, u32[]{:S(2)}, u32[]{:S(2)}) %all-to-all-start.1) | async-done | bytes 524320 | tf_op jit(solution)/shard_map/all_to_all | solution.py:141
  80.3 2.3 fusion.10
  82.7 0.8 copy.202
  83.5 4.8 %all-to-all-start.4 = ((bf16[16,16,320]{2,1,0:T(8,128)(2,1)}), bf16[16,16,320]{2,1,0:T(8,128)(2,1)S(1)}, u32[]{:S(2)}, u32[]{:S(2)}) async-start(bf16[16,16,320]{2,1,0:T(8,128)(2,1)} %bitcast.25), calls=%async_computation.4 | async-start | bytes 393216 | tf_op jit(solution)/shard_map/all_to_all | solution.py:150
  88.5 7.9 %all-to-all-done.4 = bf16[16,16,320]{2,1,0:T(8,128)(2,1)S(1)} async-done(((bf16[16,16,320]{2,1,0:T(8,128)(2,1)}), bf16[16,16,320]{2,1,0:T(8,128)(2,1)S(1)}, u32[]{:S(2)}, u32[]{:S(2)}) %all-to-all-start.4) | async-done | bytes 163872 | tf_op jit(solution)/shard_map/all_to_all | solution.py:150
  98.2 1.1 fusion.9
  99.3 1.3 fusion.14
  100.6 7.6 %multiply_add_fusion = f32[4,32,64,128]{3,2,1,0:T(8,128)S(1)} fusion(f32[4,32,64,128]{3,2,1,0:T(8,128)S(1)} %copy-done.2, f32[4,4,32,128]{3,1,2,0:T(4,128)S(1)} %bitcast.104, f32[4,32]{1,0:T(4,128)S(1)} %exp.62, f32[4,4,32,64]{3,2,1,0:T(8,128)S(1)} %reshape.159, f32[4,4,32]{1,2,0:T(8,128)S(1)} %copy.187), kind=kOutput, calls=%fused_computation.3 | convolution fusion | flops 52461568 | bytes 8784384 | tf_op jit(solution)/shard_map/vmap(sh,shp,shn->hpn)/dot_general | solution.py:60
  108.2 2.0 copy-done.1
  110.2 6.8 %fusion.67 = f32[4,32,64,4]{2,3,1,0:T(4,128)S(1)} fusion(f32[4,32,64,128]{3,2,1,0:T(8,128)S(1)} %multiply_add_fusion, f32[4,4,32,128]{3,1,2,0:T(4,128)S(1)} %bitcast.103), kind=kOutput, calls=%fused_computation.121 | convolution fusion | flops 50331648 | bytes 4587520 | tf_op jit(solution)/shard_map/vmap(thn,hpn->thp)/dot_general | solution.py:85
  117.9 103.2 %all-gather.5.cloned.1.call-done = bf16[2048,2048]{1,0:T(8,128)(2,1)} async-done(((bf16[2048,128]{1,0:T(8,128)(2,1)}), bf16[2048,2048]{1,0:T(8,128)(2,1)}) %all-gather.5.cloned.1.call-update) | async-done | bytes 8388624 | tf_op jit(solution)/shard_map/all_gather | solution.py:187
  221.0 5.2 %convolution_convert_fusion = bf16[16,2048]{1,0:T(8,128)(2,1)} fusion(bf16[2048,2048]{1,0:T(8,128)(2,1)} %all-gather.5.cloned.1.call-done, f32[16,2048]{1,0:T(8,128)S(1)} %bitcast.105, f32[16,2048]{1,0:T(8,128)S(1)} %reshape.169, f32[16,2,8,128]{3,2,1,0:T(8,128)S(1)} %get-tuple-element.40, f32[2048]{0:T(1024)S(1)} %copy-done.11), kind=kOutput, calls=%fused_computation.4 | convolution fusion | flops 134512640 | bytes 8855552 | tf_op jit(solution)/shard_map/dot_general | solution.py:185
  226.3 0.7 copy.222
  228.3 3.9 %reduce-scatter.2.cloned.1.call-done = bf16[16,1024]{1,0:T(8,128)(2,1)} async-done(((bf16[16,2048]{1,0:T(8,128)(2,1)}), bf16[16,1024]{1,0:T(8,128)(2,1)}) %reduce-scatter.2.cloned.1.call-update) | async-done | bytes 32784 | tf_op jit(solution)/shard_map/reduce_scatter | solution.py:190
  232.2 1.4 reshape.170
  (99 shorter events, 7.0 us)
Async XLA Ops:
  7.2 38.9 %copy-start = (bf16[2048,64]{0,1:T(8,128)(2,1)S(1)}, bf16[2048,64]{0,1:T(8,128)(2,1)}, u32[]{:S(2)}) copy-start(bf16[2048,64]{0,1:T(8,128)(2,1)} %param.27) | copy-start | bytes 786436
  7.2 37.8 %copy-start.7 = (bf16[128,2048]{1,0:T(8,128)(2,1)S(1)}, bf16[128,2048]{1,0:T(8,128)(2,1)}, u32[]{:S(2)}) copy-start(bf16[128,2048]{1,0:T(8,128)(2,1)} %param.24) | copy-start | bytes 1572868
  7.2 38.8 %copy-start.17 = (s32[4]{0:T(128)S(1)}, s32[4]{0:T(128)}, u32[]{:S(2)}) copy-start(s32[4]{0:T(128)} %param.41) | copy-start | bytes 52
  7.2 38.8 %copy-start.16 = (f32[32]{0:T(128)S(1)}, f32[32]{0:T(128)}, u32[]{:S(2)}) copy-start(f32[32]{0:T(128)} %param.32) | copy-start | bytes 388
  7.2 39.0 %copy-start.14 = (f32[32]{0:T(128)S(1)}, f32[32]{0:T(128)}, u32[]{:S(2)}) copy-start(f32[32]{0:T(128)} %param.31) | copy-start | bytes 388
  7.2 39.0 %copy-start.10 = (bf16[4,4,32]{2,1,0:T(4,128)(2,1)S(1)}, bf16[4,4,32]{2,1,0:T(4,128)(2,1)}, u32[]{:S(2)}) copy-start(bf16[4,4,32]{2,1,0:T(4,128)(2,1)} %param.40) | copy-start | bytes 3076
  7.2 56.5 %copy-start.3 = (bf16[4,7,2048]{2,0,1:T(4,128)(2,1)S(1)}, bf16[4,7,2048]{2,0,1:T(4,128)(2,1)}, u32[]{:S(2)}) copy-start(bf16[4,7,2048]{2,0,1:T(4,128)(2,1)} %param.37) | copy-start | bytes 344068
  7.2 57.4 %copy-start.4 = (bf16[4,7,512]{2,0,1:T(4,128)(2,1)S(1)}, bf16[4,7,512]{2,0,1:T(4,128)(2,1)}, u32[]{:S(2)}) copy-start(bf16[4,7,512]{2,0,1:T(4,128)(2,1)} %param.38) | copy-start | bytes 86020
  7.3 58.3 %copy-start.5 = (bf16[4,7,512]{2,0,1:T(4,128)(2,1)S(1)}, bf16[4,7,512]{2,0,1:T(4,128)(2,1)}, u32[]{:S(2)}) copy-start(bf16[4,7,512]{2,0,1:T(4,128)(2,1)} %param.39) | copy-start | bytes 86020
  7.3 59.0 %copy-start.12 = (f32[4,512]{1,0:T(4,128)S(1)}, f32[4,512]{1,0:T(4,128)}, u32[]{:S(2)}) copy-start(f32[4,512]{1,0:T(4,128)} %param.29) | copy-start | bytes 24580
  7.3 59.1 %copy-start.8 = (f32[4,2048]{1,0:T(4,128)S(1)}, f32[4,2048]{1,0:T(4,128)}, u32[]{:S(2)}) copy-start(f32[4,2048]{1,0:T(4,128)} %param.28) | copy-start | bytes 98308
  7.3 73.1 %all-gather.3.cloned.1.call-start = ((), (), s32[]{:S(2)}) async-start(), calls=%async_computation.6 | async-start | bytes 1114112 | tf_op jit(solution)/shard_map/all_gather | solution.py:148
  11.3 34.8 %copy-start.6 = (bf16[16,2048]{1,0:T(8,128)(2,1)S(1)}, bf16[16,2048]{1,0:T(8,128)(2,1)}, u32[]{:S(2)}) copy-start(bf16[16,2048]{1,0:T(8,128)(2,1)} %reshape.162) | copy-start | bytes 196612
  11.3 209.8 %all-gather.5.cloned.1.call-start = ((), (), s32[]{:S(2)}) async-start(), calls=%async_computation.7 | async-start | bytes 8912896 | tf_op jit(solution)/shard_map/all_gather | solution.py:187
  13.7 16.4 %all-to-all-start.2 = ((bf16[128,16,32]{0,2,1:T(8,128)(2,1)}), bf16[128,16,32]{0,2,1:T(8,128)(2,1)S(1)}, u32[]{:S(2)}, u32[]{:S(2)}) async-start(bf16[128,16,32]{0,2,1:T(8,128)(2,1)} %bitcast.19), calls=%async_computation.2 | async-start | bytes 262144 | tf_op jit(solution)/shard_map/all_to_all | solution.py:142
  30.1 11.3 %all-to-all-start.3 = ((bf16[128,16,32]{0,2,1:T(8,128)(2,1)}), bf16[128,16,32]{0,2,1:T(8,128)(2,1)S(1)}, u32[]{:S(2)}, u32[]{:S(2)}) async-start(bf16[128,16,32]{0,2,1:T(8,128)(2,1)} %bitcast.22), calls=%async_computation.3 | async-start | bytes 262144 | tf_op jit(solution)/shard_map/all_to_all | solution.py:143
  41.4 18.3 %all-to-all-start = ((bf16[128,16,128]{0,2,1:T(8,128)(2,1)}), bf16[128,16,128]{0,2,1:T(8,128)(2,1)S(1)}, u32[]{:S(2)}, u32[]{:S(2)}) async-start(bf16[128,16,128]{0,2,1:T(8,128)(2,1)} %bitcast.13), calls=%async_computation | async-start | bytes 1048576 | tf_op jit(solution)/shard_map/all_to_all | solution.py:140
  46.2 36.4 %copy-start.9 = (bf16[16,32]{1,0:T(8,128)(2,1)}, bf16[16,32]{1,0:T(8,128)(2,1)S(1)}, u32[]{:S(2)}) copy-start(bf16[16,32]{1,0:T(8,128)(2,1)S(1)} %convolution_convert_fusion.1) | copy-start | bytes 3076
  59.6 20.4 %all-to-all-start.1 = ((bf16[128,16,128]{0,2,1:T(8,128)(2,1)}), bf16[128,16,128]{0,2,1:T(8,128)(2,1)S(1)}, u32[]{:S(2)}, u32[]{:S(2)}) async-start(bf16[128,16,128]{0,2,1:T(8,128)(2,1)} %bitcast.16), calls=%async_computation.1 | async-start | bytes 1048576 | tf_op jit(solution)/shard_map/all_to_all | solution.py:141
  80.0 8.5 %copy-start.13 = (f32[4,512]{1,0:T(4,128)S(1)}, f32[4,512]{1,0:T(4,128)}, u32[]{:S(2)}) copy-start(f32[4,512]{1,0:T(4,128)} %param.30) | copy-start | bytes 24580
  83.5 13.0 %all-to-all-start.4 = ((bf16[16,16,320]{2,1,0:T(8,128)(2,1)}), bf16[16,16,320]{2,1,0:T(8,128)(2,1)S(1)}, u32[]{:S(2)}, u32[]{:S(2)}) async-start(bf16[16,16,320]{2,1,0:T(8,128)(2,1)} %bitcast.25), calls=%async_computation.4 | async-start | bytes 393216 | tf_op jit(solution)/shard_map/all_to_all | solution.py:150
  88.3 143.9 %reduce-scatter.2.cloned.1.call-start = ((), (), s32[]{:S(2)}) async-start(), calls=%async_computation.8 | async-start | bytes 98304 | tf_op jit(solution)/shard_map/reduce_scatter | solution.py:190
  97.9 2.7 %copy-start.2 = (f32[4,32,64,128]{3,2,1,0:T(8,128)S(1)}, f32[4,32,64,128]{3,2,1,0:T(8,128)}, u32[]{:S(2)}) copy-start(f32[4,32,64,128]{3,2,1,0:T(8,128)} %param.36) | copy-start | bytes 12582916
  108.2 2.0 copy-start.1
  110.2 6.8 %copy-start.15 = (f32[32]{0:T(128)S(1)}, f32[32]{0:T(128)}, u32[]{:S(2)}) copy-start(f32[32]{0:T(128)} %param.33) | copy-start | bytes 388
  110.2 110.8 %copy-start.11 = (f32[2048]{0:T(1024)S(1)}, f32[2048]{0:T(1024)}, u32[]{:S(2)}) copy-start(f32[2048]{0:T(1024)} %param.34) | copy-start | bytes 24580
Sparse Core Ops, SparseCore 0:
  11.4 63.3 all-gather.2
  77.5 143.4 all-gather.4
  226.4 5.7 reduce-scatter.1
where the time goes:
time: 241 us; the launch traced here: 240 us
  waiting for transfers between devices  154 us (64%)
  matrix products  24.4 us (10%)
  starting transfers between devices  24.3 us (10%)
  local copies, waits for them, and re-layouts  18.5 us (8%)
  between operations  14.2 us (6%)
    all_gather x1, waiting for transfers between devices, on_device(): lax.all_gather(out_weight, 'kv', axis=1, tiled=True)  103 us
    all_to_all x1, waiting for transfers between devices, on_device(): lax.all_to_all(gate_weight, 'kv', split_axis=1, concat_axis=0, tiled=True)  13.3 us
    all_to_all x1, waiting for transfers between devices, on_device(): lax.all_to_all(value_weight, 'kv', split_axis=1, concat_axis=0, tiled=True)  12.8 us
    unnamed x45, local copies, waits for them, and re-layouts  10.6 us
    all_to_all x1, starting transfers between devices, on_device(): lax.all_to_all(write_weight, 'kv', split_axis=1, concat_axis=0, tiled=True)  8.2 us
    all_to_all x1, waiting for transfers between devices, on_device(): lax.all_to_all(everyone, 'kv', split_axis=0, concat_axis=1, tiled=True)  7.89 us
    dot_general x1, matrix products, advance(): jnp.einsum('sh,shp,shn->hpn', weight_now, prev_x, prev_b, precision=highest)  7.61 us
    dot_general x1, matrix products, advance(): jnp.einsum('thn,hpn->thp', cur_c, root, precision=highest)  6.79 us
  transfers between devices with their start and end apart: 8, of which 7 were waited for; matrix products, arithmetic and copies ran while one was open for 15% of the time, Pallas kernels for 0%

commit v1 on v0

--- a/solution.py
+++ b/solution.py
@@ -184,7 +184,7 @@
     flat_y = normal_out.reshape(token_count, -1)
     partial_sum = jnp.dot(
         flat_y,
-        lax.all_gather(out_weight, "kv", axis=1, tiled=True),
+        jnp.concatenate(lax.all_gather(out_weight, "kv"), axis=1),
         preferred_element_type=jnp.float32,
     )
     summed = lax.psum_scatter(

time: 241 us -> 227 us (0.942)
  waiting for transfers between devices: 154 us -> 126 us
  local copies, waits for them, and re-layouts: 18.5 us -> 30.5 us
    all_gather x1, waiting for transfers between devices: 103 us -> 71.4 us  [on_device(): lax.all_gather(out_weight, 'kv')]
    reshape x0 -> x1, local copies, waits for them, and re-layouts: none -> 12 us  [on_device(): jnp.concatenate(lax.all_gather(out_weight, 'kv'), axis=1)]
    all_to_all x1, waiting for transfers between devices: 7.89 us -> 11.8 us  [on_device(): lax.all_to_all(everyone, 'kv', split_axis=0, concat_axis=1, tiled=True)]
  transfers between devices with their start and end apart: 8 -> 8, of which waited for: 7 -> 7; matrix products, arithmetic and copies ran while one was open for 15% -> 16% of each run, Pallas kernels for 0% -> 0%
where the time goes in v1:
time: 227 us; the launch traced here: 225 us
  waiting for transfers between devices  126 us (56%)
  local copies, waits for them, and re-layouts  30.5 us (13%)
  matrix products  25.5 us (11%)
  starting transfers between devices  24.3 us (11%)
  between operations  14.3 us (6%)
  other arithmetic  2.4 us (1%)
  blocking collectives  2.34 us (1%)
    all_gather x1, waiting for transfers between devices, on_device(): lax.all_gather(out_weight, 'kv')  71.4 us
    all_to_all x1, waiting for transfers between devices, on_device(): lax.all_to_all(gate_weight, 'kv', split_axis=1, concat_axis=0, tiled=True)  13.3 us
    all_to_all x1, waiting for transfers between devices, on_device(): lax.all_to_all(value_weight, 'kv', split_axis=1, concat_axis=0, tiled=True)  12.8 us
    reshape x1, local copies, waits for them, and re-layouts, on_device(): jnp.concatenate(lax.all_gather(out_weight, 'kv'), axis=1)  12 us
    all_to_all x1, waiting for transfers between devices, on_device(): lax.all_to_all(everyone, 'kv', split_axis=0, concat_axis=1, tiled=True)  11.8 us
    unnamed x45, local copies, waits for them, and re-layouts  10.6 us
    all_to_all x1, starting transfers between devices, on_device(): lax.all_to_all(write_weight, 'kv', split_axis=1, concat_axis=0, tiled=True)  8.2 us
    dot_general x1, matrix products, advance(): jnp.einsum('sh,shp,shn->hpn', weight_now, prev_x, prev_b, precision=highest)  7.61 us
  transfers between devices with their start and end apart: 8, of which 7 were waited for; matrix products, arithmetic and copies ran while one was open for 16% of the time, Pallas kernels for 0%

profile of v1, /device:TPU:0, one launch (start us, length us, event | category | flops | bytes accessed | tf_op | source)
XLA Modules:
  0.0 225.4 jit_solution(8584618440573531595)
XLA Ops:
  7.3 2.3 %all_gather.12 = bf16[4,4,2048]{2,1,0:T(4,128)(2,1)S(1)} all-gather(bf16[4,4,1024]{2,1,0:T(4,128)(2,1)} %param.21), channel_id=1, replica_groups=mesh['kv'=16,'tp'=2] {'tp'}, dimensions={2}, use_global_device_ids=true | all-gather | bytes 98304 | tf_op jit(solution)/shard_map/all_gather | solution.py:126
  9.8 0.8 fusion.19
  10.6 0.6 reshape.215
  11.3 0.7 all-gather.6.cloned.1.call-update
  12.1 1.7 copy.199
  13.7 8.2 %all-to-all-start.2 = ((bf16[128,16,32]{0,2,1:T(8,128)(2,1)}), bf16[128,16,32]{0,2,1:T(8,128)(2,1)S(1)}, u32[]{:S(2)}, u32[]{:S(2)}) async-start(bf16[128,16,32]{0,2,1:T(8,128)(2,1)} %bitcast.19), calls=%async_computation.2 | async-start | bytes 262144 | tf_op jit(solution)/shard_map/all_to_all | solution.py:142
  21.9 1.7 copy.201
  23.6 6.5 %all-to-all-done.2 = bf16[128,16,32]{0,2,1:T(8,128)(2,1)S(1)} async-done(((bf16[128,16,32]{0,2,1:T(8,128)(2,1)}), bf16[128,16,32]{0,2,1:T(8,128)(2,1)S(1)}, u32[]{:S(2)}, u32[]{:S(2)}) %all-to-all-start.2) | async-done | bytes 131104 | tf_op jit(solution)/shard_map/all_to_all | solution.py:142
  30.1 3.5 %all-to-all-start.3 = ((bf16[128,16,32]{0,2,1:T(8,128)(2,1)}), bf16[128,16,32]{0,2,1:T(8,128)(2,1)S(1)}, u32[]{:S(2)}, u32[]{:S(2)}) async-start(bf16[128,16,32]{0,2,1:T(8,128)(2,1)} %bitcast.22), calls=%async_computation.3 | async-start | bytes 262144 | tf_op jit(solution)/shard_map/all_to_all | solution.py:143
  33.6 2.0 copy.195
  35.7 5.7 %all-to-all-done.3 = bf16[128,16,32]{0,2,1:T(8,128)(2,1)S(1)} async-done(((bf16[128,16,32]{0,2,1:T(8,128)(2,1)}), bf16[128,16,32]{0,2,1:T(8,128)(2,1)S(1)}, u32[]{:S(2)}, u32[]{:S(2)}) %all-to-all-start.3) | async-done | bytes 131104 | tf_op jit(solution)/shard_map/all_to_all | solution.py:143
  41.4 3.6 %all-to-all-start = ((bf16[128,16,128]{0,2,1:T(8,128)(2,1)}), bf16[128,16,128]{0,2,1:T(8,128)(2,1)S(1)}, u32[]{:S(2)}, u32[]{:S(2)}) async-start(bf16[128,16,128]{0,2,1:T(8,128)(2,1)} %bitcast.13), calls=%async_computation | async-start | bytes 1048576 | tf_op jit(solution)/shard_map/all_to_all | solution.py:140
  45.0 1.0 copy.197
  46.3 13.3 %all-to-all-done = bf16[128,16,128]{0,2,1:T(8,128)(2,1)S(1)} async-done(((bf16[128,16,128]{0,2,1:T(8,128)(2,1)}), bf16[128,16,128]{0,2,1:T(8,128)(2,1)S(1)}, u32[]{:S(2)}, u32[]{:S(2)}) %all-to-all-start) | async-done | bytes 524320 | tf_op jit(solution)/shard_map/all_to_all | solution.py:140
  59.7 3.9 %all-to-all-start.1 = ((bf16[128,16,128]{0,2,1:T(8,128)(2,1)}), bf16[128,16,128]{0,2,1:T(8,128)(2,1)S(1)}, u32[]{:S(2)}, u32[]{:S(2)}) async-start(bf16[128,16,128]{0,2,1:T(8,128)(2,1)} %bitcast.16), calls=%async_computation.1 | async-start | bytes 1048576 | tf_op jit(solution)/shard_map/all_to_all | solution.py:141
  65.1 0.8 gather_fusion.1
  67.3 12.8 %all-to-all-done.1 = bf16[128,16,128]{0,2,1:T(8,128)(2,1)S(1)} async-done(((bf16[128,16,128]{0,2,1:T(8,128)(2,1)}), bf16[128,16,128]{0,2,1:T(8,128)(2,1)S(1)}, u32[]{:S(2)}, u32[]{:S(2)}) %all-to-all-start.1) | async-done | bytes 524320 | tf_op jit(solution)/shard_map/all_to_all | solution.py:141
  80.4 2.3 %fusion.10 = bf16[256,320]{0,1:T(8,128)(2,1)S(1)} fusion(bf16[256,2048]{1,0:T(8,128)(2,1)} %all-gather.4.cloned.1.call-done, bf16[2048,32]{1,0:T(8,128)(2,1)S(1)} %bitcast.90, bf16[2048,32]{1,0:T(8,128)(2,1)S(1)} %bitcast.91, bf16[2048,128]{1,0:T(8,128)(2,1)S(1)} %bitcast.95, bf16[2048,128]{1,0:T(8,128)(2,1)S(1)} %bitcast.94), kind=kOutput, calls=%fused_computation.16 | convolution fusion | flops 340869120 | bytes 2523136 | tf_op jit(solution)/shard_map/dot_general | solution.py:147
  82.7 0.8 copy.205
  83.5 4.8 %all-to-all-start.4 = ((bf16[16,16,320]{2,1,0:T(8,128)(2,1)}), bf16[16,16,320]{2,1,0:T(8,128)(2,1)S(1)}, u32[]{:S(2)}, u32[]{:S(2)}) async-start(bf16[16,16,320]{2,1,0:T(8,128)(2,1)} %bitcast.25), calls=%async_computation.4 | async-start | bytes 393216 | tf_op jit(solution)/shard_map/all_to_all | solution.py:150
  88.6 11.8 %all-to-all-done.4 = bf16[16,16,320]{2,1,0:T(8,128)(2,1)S(1)} async-done(((bf16[16,16,320]{2,1,0:T(8,128)(2,1)}), bf16[16,16,320]{2,1,0:T(8,128)(2,1)S(1)}, u32[]{:S(2)}, u32[]{:S(2)}) %all-to-all-start.4) | async-done | bytes 163872 | tf_op jit(solution)/shard_map/all_to_all | solution.py:150
  102.2 1.1 fusion.9
  103.3 1.3 fusion.14
  104.6 7.6 %multiply_add_fusion = f32[4,32,64,128]{3,2,1,0:T(8,128)S(1)} fusion(f32[4,32,64,128]{3,2,1,0:T(8,128)S(1)} %copy-done.2, f32[4,4,32,128]{3,1,2,0:T(4,128)S(1)} %bitcast.89, f32[4,32]{1,0:T(4,128)S(1)} %exp.69, f32[4,4,32,64]{3,2,1,0:T(8,128)S(1)} %reshape.212, f32[4,4,32]{1,2,0:T(8,128)S(1)} %copy.190), kind=kOutput, calls=%fused_computation.3 | convolution fusion | flops 52461568 | bytes 8784384 | tf_op jit(solution)/shard_map/vmap(sh,shp,shn->hpn)/dot_general | solution.py:60
  112.2 2.0 copy-done.1
  114.2 6.8 %fusion.57 = f32[4,32,64,4]{2,3,1,0:T(4,128)S(1)} fusion(f32[4,32,64,128]{3,2,1,0:T(8,128)S(1)} %multiply_add_fusion, f32[4,4,32,128]{3,1,2,0:T(4,128)S(1)} %bitcast.88), kind=kOutput, calls=%fused_computation.112 | convolution fusion | flops 50331648 | bytes 4587520 | tf_op jit(solution)/shard_map/vmap(thn,hpn->thp)/dot_general | solution.py:85
  121.9 71.4 %all-gather.6.cloned.1.call-done = bf16[32768,128]{1,0:T(8,128)(2,1)} async-done(((bf16[2048,128]{1,0:T(8,128)(2,1)}), bf16[32768,128]{1,0:T(8,128)(2,1)}) %all-gather.6.cloned.1.call-update) | async-done | bytes 8388624 | tf_op jit(solution)/shard_map/all_gather | solution.py:187
  193.3 12.0 %copy.225 = bf16[2048,16,128]{0,2,1:T(8,128)(2,1)} copy(bf16[2048,16,128]{2,0,1:T(8,128)(2,1)} %bitcast.82) | data formatting | bytes 16777216 | tf_op jit(solution)/shard_map/reshape | solution.py:187
  205.3 6.3 %convolution_convert_fusion = bf16[16,2048]{1,0:T(8,128)(2,1)} fusion(bf16[16,2048]{1,0:T(8,128)(2,1)S(1)} %bitcast.96, bf16[2048,2048]{0,1:T(8,128)(2,1)} %bitcast.81), kind=kOutput, calls=%fused_computation.4 | convolution fusion | flops 134250496 | bytes 8519680 | tf_op jit(solution)/shard_map/dot_general | solution.py:185
  212.9 0.7 copy.226
  213.6 3.9 %reduce-scatter.2.cloned.1.call-done = bf16[16,1024]{1,0:T(8,128)(2,1)} async-done(((bf16[16,2048]{1,0:T(8,128)(2,1)}), bf16[16,1024]{1,0:T(8,128)(2,1)}) %reduce-scatter.2.cloned.1.call-update) | async-done | bytes 32784 | tf_op jit(solution)/shard_map/reduce_scatter | solution.py:190
  217.5 1.4 reshape.225
  (102 shorter events, 7.8 us)
Async XLA Ops:
  7.2 38.9 %copy-start = (bf16[2048,64]{0,1:T(8,128)(2,1)S(1)}, bf16[2048,64]{0,1:T(8,128)(2,1)}, u32[]{:S(2)}) copy-start(bf16[2048,64]{0,1:T(8,128)(2,1)} %param.27) | copy-start | bytes 786436
  7.2 37.8 %copy-start.7 = (bf16[128,2048]{1,0:T(8,128)(2,1)S(1)}, bf16[128,2048]{1,0:T(8,128)(2,1)}, u32[]{:S(2)}) copy-start(bf16[128,2048]{1,0:T(8,128)(2,1)} %param.24) | copy-start | bytes 1572868
  7.2 38.8 %copy-start.17 = (s32[4]{0:T(128)S(1)}, s32[4]{0:T(128)}, u32[]{:S(2)}) copy-start(s32[4]{0:T(128)} %param.41) | copy-start | bytes 52
  7.2 38.8 %copy-start.16 = (f32[32]{0:T(128)S(1)}, f32[32]{0:T(128)}, u32[]{:S(2)}) copy-start(f32[32]{0:T(128)} %param.32) | copy-start | bytes 388
  7.2 39.0 %copy-start.10 = (bf16[4,4,32]{2,1,0:T(4,128)(2,1)S(1)}, bf16[4,4,32]{2,1,0:T(4,128)(2,1)}, u32[]{:S(2)}) copy-start(bf16[4,4,32]{2,1,0:T(4,128)(2,1)} %param.40) | copy-start | bytes 3076
  7.2 39.0 %copy-start.14 = (f32[32]{0:T(128)S(1)}, f32[32]{0:T(128)}, u32[]{:S(2)}) copy-start(f32[32]{0:T(128)} %param.31) | copy-start | bytes 388
  7.2 56.5 %copy-start.11 = (f32[2048]{0:T(1024)S(1)}, f32[2048]{0:T(1024)}, u32[]{:S(2)}) copy-start(f32[2048]{0:T(1024)} %param.34) | copy-start | bytes 24580
  7.2 56.5 %copy-start.4 = (bf16[4,7,512]{2,0,1:T(4,128)(2,1)S(1)}, bf16[4,7,512]{2,0,1:T(4,128)(2,1)}, u32[]{:S(2)}) copy-start(bf16[4,7,512]{2,0,1:T(4,128)(2,1)} %param.38) | copy-start | bytes 86020
  7.3 57.2 %copy-start.5 = (bf16[4,7,512]{2,0,1:T(4,128)(2,1)S(1)}, bf16[4,7,512]{2,0,1:T(4,128)(2,1)}, u32[]{:S(2)}) copy-start(bf16[4,7,512]{2,0,1:T(4,128)(2,1)} %param.39) | copy-start | bytes 86020
  7.3 57.9 %copy-start.3 = (bf16[4,7,2048]{2,0,1:T(4,128)(2,1)S(1)}, bf16[4,7,2048]{2,0,1:T(4,128)(2,1)}, u32[]{:S(2)}) copy-start(bf16[4,7,2048]{2,0,1:T(4,128)(2,1)} %param.37) | copy-start | bytes 344068
  7.3 59.1 %copy-start.12 = (f32[4,512]{1,0:T(4,128)S(1)}, f32[4,512]{1,0:T(4,128)}, u32[]{:S(2)}) copy-start(f32[4,512]{1,0:T(4,128)} %param.29) | copy-start | bytes 24580
  7.3 59.1 %copy-start.8 = (f32[4,2048]{1,0:T(4,128)S(1)}, f32[4,2048]{1,0:T(4,128)}, u32[]{:S(2)}) copy-start(f32[4,2048]{1,0:T(4,128)} %param.28) | copy-start | bytes 98308
  7.3 73.1 %all-gather.4.cloned.1.call-start = ((), (), s32[]{:S(2)}) async-start(), calls=%async_computation.6 | async-start | bytes 1114112 | tf_op jit(solution)/shard_map/all_gather | solution.py:148
  11.3 34.8 %copy-start.6 = (bf16[16,2048]{1,0:T(8,128)(2,1)S(1)}, bf16[16,2048]{1,0:T(8,128)(2,1)}, u32[]{:S(2)}) copy-start(bf16[16,2048]{1,0:T(8,128)(2,1)} %reshape.215) | copy-start | bytes 196612
  11.3 182.0 %all-gather.6.cloned.1.call-start = ((), (), s32[]{:S(2)}) async-start(), calls=%async_computation.8 | async-start | bytes 8912896 | tf_op jit(solution)/shard_map/all_gather | solution.py:187
  13.7 16.4 %all-to-all-start.2 = ((bf16[128,16,32]{0,2,1:T(8,128)(2,1)}), bf16[128,16,32]{0,2,1:T(8,128)(2,1)S(1)}, u32[]{:S(2)}, u32[]{:S(2)}) async-start(bf16[128,16,32]{0,2,1:T(8,128)(2,1)} %bitcast.19), calls=%async_computation.2 | async-start | bytes 262144 | tf_op jit(solution)/shard_map/all_to_all | solution.py:142
  30.1 11.3 %all-to-all-start.3 = ((bf16[128,16,32]{0,2,1:T(8,128)(2,1)}), bf16[128,16,32]{0,2,1:T(8,128)(2,1)S(1)}, u32[]{:S(2)}, u32[]{:S(2)}) async-start(bf16[128,16,32]{0,2,1:T(8,128)(2,1)} %bitcast.22), calls=%async_computation.3 | async-start | bytes 262144 | tf_op jit(solution)/shard_map/all_to_all | solution.py:143
  41.4 18.3 %all-to-all-start = ((bf16[128,16,128]{0,2,1:T(8,128)(2,1)}), bf16[128,16,128]{0,2,1:T(8,128)(2,1)S(1)}, u32[]{:S(2)}, u32[]{:S(2)}) async-start(bf16[128,16,128]{0,2,1:T(8,128)(2,1)} %bitcast.13), calls=%async_computation | async-start | bytes 1048576 | tf_op jit(solution)/shard_map/all_to_all | solution.py:140
  46.2 36.4 %copy-start.9 = (bf16[16,32]{1,0:T(8,128)(2,1)}, bf16[16,32]{1,0:T(8,128)(2,1)S(1)}, u32[]{:S(2)}) copy-start(bf16[16,32]{1,0:T(8,128)(2,1)S(1)} %convolution_convert_fusion.1) | copy-start | bytes 3076
  59.7 20.4 %all-to-all-start.1 = ((bf16[128,16,128]{0,2,1:T(8,128)(2,1)}), bf16[128,16,128]{0,2,1:T(8,128)(2,1)S(1)}, u32[]{:S(2)}, u32[]{:S(2)}) async-start(bf16[128,16,128]{0,2,1:T(8,128)(2,1)} %bitcast.16), calls=%async_computation.1 | async-start | bytes 1048576 | tf_op jit(solution)/shard_map/all_to_all | solution.py:141
  80.0 8.5 %copy-start.13 = (f32[4,512]{1,0:T(4,128)S(1)}, f32[4,512]{1,0:T(4,128)}, u32[]{:S(2)}) copy-start(f32[4,512]{1,0:T(4,128)} %param.30) | copy-start | bytes 24580
  83.5 16.9 %all-to-all-start.4 = ((bf16[16,16,320]{2,1,0:T(8,128)(2,1)}), bf16[16,16,320]{2,1,0:T(8,128)(2,1)S(1)}, u32[]{:S(2)}, u32[]{:S(2)}) async-start(bf16[16,16,320]{2,1,0:T(8,128)(2,1)} %bitcast.25), calls=%async_computation.4 | async-start | bytes 393216 | tf_op jit(solution)/shard_map/all_to_all | solution.py:150
  88.3 129.2 %reduce-scatter.2.cloned.1.call-start = ((), (), s32[]{:S(2)}) async-start(), calls=%async_computation.7 | async-start | bytes 98304 | tf_op jit(solution)/shard_map/reduce_scatter | solution.py:190
  101.9 2.7 %copy-start.2 = (f32[4,32,64,128]{3,2,1,0:T(8,128)S(1)}, f32[4,32,64,128]{3,2,1,0:T(8,128)}, u32[]{:S(2)}) copy-start(f32[4,32,64,128]{3,2,1,0:T(8,128)} %param.36) | copy-start | bytes 12582916
  112.2 2.0 copy-start.1
  114.2 6.8 %copy-start.15 = (f32[32]{0:T(128)S(1)}, f32[32]{0:T(128)}, u32[]{:S(2)}) copy-start(f32[32]{0:T(128)} %param.33) | copy-start | bytes 388
Sparse Core Ops, SparseCore 0:
  11.4 63.3 all-gather.3
  77.6 115.6 all-gather.5
  211.7 5.7 reduce-scatter.1
